TPU v7x, 512 devices: a 4x2x32 block of a 4x8x32 slice. The times are simulated.
512 devices in a mesh: grp: 2 (over y), fs: 32 (over z), tp: 8 (over x, core).
Axes of the slice: x: 4, y: 2, z: 32, core: 2. Of those that a mesh axis runs over, the one named last changes fastest.
The devices are a block of a 4x8x32 slice.
Arguments:
- layer_input_tokens: bfloat16 [32768, 2048], P(('grp', 'fs')), parts along dimension 0, may hold values from -6 to 6
- attention_norm_gain: float32 [2048], replicated, may hold values from 0.1 to 1.9
- query_projection: bfloat16 [2048, 1024], P('fs', 'tp'), may hold values from -0.125 to 0.125
- key_projection: bfloat16 [2048, 1024], P('fs', 'tp'), may hold values from -0.125 to 0.125
- value_projection: bfloat16 [2048, 2048], P('fs', 'tp'), may hold values from -0.125 to 0.125
- decay_first_factor: bfloat16 [2048, 16], replicated, may hold values from -0.125 to 0.125
- decay_second_factor: bfloat16 [16, 1024], P(None, 'tp'), may hold values from -1.5 to 1.5
- decay_logit_bias: float32 [1024], P('tp'), may hold values from -0.5 to 6
- extra_log_decay: float32 [32768, 8], P(('grp', 'fs'), 'tp'), parts along dimension 0, may hold values from -0.7 to 0
- head_output_gain: float32 [256], replicated, may hold values from 0.1 to 1.9
- attention_output_projection: bfloat16 [2048, 2048], P(('tp', 'fs')), may hold values from -0.125 to 0.125
- feedforward_norm_gain: float32 [2048], replicated, may hold values from 0.1 to 1.9
- gate_projection: bfloat16 [2048, 5632], P('fs', 'tp'), may hold values from -0.125 to 0.125
- up_projection: bfloat16 [2048, 5632], P('fs', 'tp'), may hold values from -0.125 to 0.125
- down_projection: bfloat16 [5632, 2048], P(('tp', 'fs')), may hold values from -0.078125 to 0.078125
Outputs:
- result: bfloat16 [32768, 2048], P(('grp', 'fs')), parts along dimension 0
There are 2 independent parts, one for each index of `grp`. A program takes and returns all parts, laid end to end along the dimension named above; an argument that names none is the same for every part. Nothing has to cross between parts.
All inputs are finite; a program needn't handle non-finite values.
Results may differ from a plain program's by a relative error of at most 0.02.
Values may be sent and summed in bfloat16 or wider, within the bound.
A program may use at most 64 MiB of HBM per device.

v0:
```python
import functools

import jax
import jax.numpy as jnp
from jax import lax
from jax.experimental import pallas as pl
from jax.experimental.pallas import tpu as pltpu
from jax.sharding import PartitionSpec as P

MESH = pl.DeviceIdType.MESH
BLOCK = 64
LANES = 128
GATE = 16.0
EPS = 1e-06
MIX_CHUNKS = 2
FF_CHUNKS = 2
VMEM_MIB = 60
GU_ROWS = (16, 16)
DN_SPLIT = (1, 1)
START = {"qkv": 0, "out": 0, "gu0": 7, "gu1": 8, "dn0": 9, "dn1": 11}
PUMP = (1, 1, 1, 1, 2, 1, 1, 1, 1)
F32 = jnp.float32
BF16 = jnp.bfloat16


def mm(a, b):
    return lax.dot_general(a, b, (((1,), (0,)), ((), ())), preferred_element_type=F32)


def mm_nt(a, b):
    return lax.dot_general(a, b, (((1,), (1,)), ((), ())), preferred_element_type=F32)


def mm_tn(a, b):
    return lax.dot_general(a, b, (((0,), (0,)), ((), ())), preferred_element_type=F32)


def iota(shape, dim):
    return lax.broadcasted_iota(jnp.int32, shape, dim)


def scaled_rows(wide, gain):
    return wide * lax.rsqrt(jnp.mean(wide * wide, axis=-1, keepdims=True) + EPS) * gain


def kernel(
    size, paired, arrived,
    x_ref, gain1_ref, wq_ref, wk_ref, wv_ref, first_ref, second_ref, bias_ref, extra_ref,
    hgain_ref, wo_ref, gain2_ref, wg_ref, wu_ref, wd_ref,
    out_ref,
    g_qkv, g_out, g_gu, g_dn,
    normed, extra_col, decs, ends, qs, ks, vs, inside, ups_f, ups_b, car, headed, wout,
    place, hid, wide_gu, mix_bufs, ff_bufs, own_res, full2, full3,
    z_send, z_recv, y_send, y_recv, ag_send, ag_recv, out_sem,
):
    n, tp = size["fs"], size["tp"]
    chips = tp // 2
    far = chips // 2
    grp, me, t = lax.axis_index("grp"), lax.axis_index("fs"), lax.axis_index("tp")
    chip, core = t // 2, t % 2
    half = grp % 2 if paired else 0
    up_z, down_z = lax.rem(me + 1, n), lax.rem(me + n - 1, n)
    twin = grp + 1 - 2 * (grp % 2)
    mate = t + 1 - 2 * core
    right, left = lax.rem(t + 2, tp), lax.rem(t + tp - 2, tp)
    rows = x_ref.shape[0]
    share = rows // tp
    blocks = rows // BLOCK
    keyw = wq_ref.shape[1]
    valw = wv_ref.shape[1]
    wide = x_ref.shape[1]
    mix_cols, cols = wide // MIX_CHUNKS, wide // FF_CHUNKS
    ffw = wg_ref.shape[1]
    whole = ffw // LANES * LANES
    rest = ffw - whole

    barrier = pltpu.get_barrier_semaphore()
    up_two, down_two = lax.rem(me + 2, n), lax.rem(me + n - 2, n)
    friends = [{"fs": z} for z in (up_z, down_z, up_two, down_two)]
    friends += [{"tp": mate}, {"tp": right}, {"tp": left}]
    if paired:
        friends.append({"grp": twin})
    for friend in friends:
        pl.semaphore_signal(barrier, inc=1, device_id=friend, device_id_type=MESH)

    arrived(range(1, 15))
    g_qkv[me, :, 0:keyw] = wq_ref[...]
    g_qkv[me, :, keyw : 2 * keyw] = wk_ref[...]
    g_qkv[me, :, 2 * keyw :] = wv_ref[...]
    g_out[me] = wo_ref[...]
    g_gu[me, :, 0:whole] = wg_ref[:, 0:whole]
    g_gu[me, :, whole : 2 * whole] = wu_ref[:, 0:whole]
    g_gu[me, :, 2 * whole :] = jnp.concatenate([wg_ref[:, whole:], wu_ref[:, whole:]], axis=1)
    dn_rows = wd_ref.shape[0]
    for c in range(FF_CHUNKS):
        g_dn[c, me] = jnp.zeros(g_dn.shape[2:], BF16)
        g_dn[c, me, 0:dn_rows, :] = wd_ref[:, c * cols : (c + 1) * cols]
    eye = iota((BLOCK, BLOCK), 0) == iota((BLOCK, BLOCK), 1)
    for b in range(blocks):
        span = slice(b * BLOCK, (b + 1) * BLOCK)
        extra_col[span, :] = jnp.sum(jnp.where(eye, extra_ref[:, span], 0.0), axis=1, keepdims=True)
    pl.semaphore_wait(barrier, len(friends))

    depth = wq_ref.shape[0]
    lot = depth // 2 if paired else depth

    def part_of(ref, first, count):
        return lambda slots: ref.at[slots, pl.ds(pl.multiple_of(half * lot + first, 8), count), :]

    QKV, OUT = "qkv", "out"
    out_cols = wide // 2 if paired else wide

    def out_part(slots):
        return g_out.at[slots, :, pl.ds(pl.multiple_of(half * out_cols, LANES), out_cols)]

    views = {QKV: part_of(g_qkv, 0, lot), OUT: out_part}
    strided = (QKV, OUT)
    GU, DN = [], []
    first = 0
    for k, count in enumerate(GU_ROWS):
        count = count * lot // sum(GU_ROWS)
        GU.append(f"gu{k}")
        views[GU[k]] = part_of(g_gu, first, count)
        first += count
    first = 0
    for k, count in enumerate(DN_SPLIT):
        views[f"dn{k}"] = lambda slots, first=first, count=count: g_dn.at[pl.ds(first, count), slots]
        DN += [f"dn{k}"] * count
        first += count
    number = {p: i for i, p in enumerate(views)}
    crossing = {p: i for i, p in enumerate([QKV, OUT] + GU)} if paired else {}
    hops = (n // 2, n - 1 - n // 2)

    def z_copy(p, way, s, view=None):
        if view is None:
            view = views[p](lax.rem(me - s + n, n) if way == 0 else lax.rem(me + s, n))
        return pltpu.make_async_remote_copy(
            src_ref=view, dst_ref=view,
            send_sem=z_send.at[number[p], way], recv_sem=z_recv.at[number[p], way, s],
            device_id={"fs": up_z if way == 0 else down_z}, device_id_type=MESH,
        )

    def y_copy(p, view):
        return pltpu.make_async_remote_copy(
            src_ref=view, dst_ref=view,
            send_sem=y_send.at[crossing[p]], recv_sem=y_recv.at[crossing[p]],
            device_id={"grp": twin}, device_id_type=MESH,
        )

    def cross(p, way, s):
        slot = lax.rem(me - s - 1 + n, n) if way == 0 else lax.rem(me + s + 1, n)
        y_copy(p, views[p](slot)).start()

    def step(p, s, ways=(0, 1), arrive=True, leave=True):
        for way in ways:
            if arrive:
                z_copy(p, way, s - 1).wait_recv()
            if leave:
                z_copy(p, way, s).start()
            if arrive and p in crossing:
                cross(p, way, s - 1)

    def away(way, distance):
        return lax.rem(me - distance + n, n) if way == 0 else lax.rem(me + distance, n)

    def far_copy(p, way, distance, two):
        view = views[p](away(way, distance))
        to = (up_two if two else up_z) if way == 0 else (down_two if two else down_z)
        return pltpu.make_async_remote_copy(
            src_ref=view, dst_ref=view, send_sem=z_send.at[number[p], way],
            recv_sem=z_recv.at[number[p], way, distance + (1 if two else 0)],
            device_id={"fs": to}, device_id_type=MESH,
        )

    def far_step(p, j):
        known = isinstance(j, int)
        for way in (0, 1):
            for distance in (2 * j - 1, 2 * j):
                if not known or distance <= hops[way]:
                    z_copy(p, way, distance - 1).wait_recv()
                    if not known or distance <= hops[way] - 2:
                        far_copy(p, way, distance, True).start()
                    if p in crossing:
                        cross(p, way, distance - 1)

    def at(p, s):
        if p in strided:
            if s > 0:
                far_step(p, s)
            else:
                for way in (0, 1):
                    far_copy(p, way, 0, False).start()
                    far_copy(p, way, 0, True).start()
            return
        for way in (0, 1):
            if s <= hops[way]:
                step(p, s, (way,), arrive=s > 0, leave=s < hops[way])

    def y_arrived(p):
        if p in crossing:
            y_copy(p, views[p](pl.ds(0, n - 1))).wait_recv()

    starts = {p: START[p] for p in views}
    order = sorted(views, key=lambda p: (starts[p], number[p]))
    clock = [0]
    final = {p: n // 4 if p in strided else n // 2 for p in views}
    even = {p: n // 4 - 1 if p in strided else hops[1] for p in views}

    def pump(count=1):
        for _ in range(count):
            tick = clock[0]
            for p in order:
                if 0 <= tick - starts[p] <= final[p]:
                    at(p, tick - starts[p])
            clock[0] += 1

    def complete(p):
        while clock[0] <= starts[p] + final[p]:
            pump()

    def glide(count, beside):
        end = clock[0] + count
        while clock[0] < end:
            tick = clock[0]
            inner = [p for p in order if 1 <= tick - starts[p] < even[p]]
            length = 0
            while tick + length < end and all(
                (1 <= tick + length - starts[p] < even[p])
                if p in inner
                else not 0 <= tick + length - starts[p] <= final[p]
                for p in order
            ):
                length += 1
            if length < 3:
                pump()
                beside(tick)
                continue

            def body(now, carry, inner=inner):
                for p in inner:
                    (far_step if p in strided else step)(p, now - starts[p])
                beside(now)
                return carry

            lax.fori_loop(tick, tick + length, body, 0)
            clock[0] += length

    def drain(p):
        for way in (0, 1):
            z_copy(p, way, 0, views[p](pl.ds(0, hops[way]))).wait_send()
        if p in crossing:
            y_copy(p, views[p](pl.ds(0, n - 1))).wait_send()

    low = iota((BLOCK, BLOCK), 0) >= iota((BLOCK, BLOCK), 1)
    high = iota((BLOCK, BLOCK), 0) <= iota((BLOCK, BLOCK), 1)

    def prepare(b):
        span = pl.ds(pl.multiple_of(b * BLOCK, BLOCK), BLOCK)
        tidy = scaled_rows(x_ref[span, :].astype(F32), gain1_ref[...]).astype(BF16)
        normed[span, :] = tidy
        lowrank = mm_nt(tidy, first_ref[...]).astype(BF16)
        logits = mm(lowrank, second_ref[...]) + bias_ref[...]
        logsig = jnp.minimum(logits, 0.0) - jnp.log1p(jnp.exp(-jnp.abs(logits)))
        dec = logsig / GATE + extra_col[span, :]
        one = dec.astype(BF16)
        left_over = dec - one.astype(F32)
        two = left_over.astype(BF16)
        three = (left_over - two.astype(F32)).astype(BF16)
        terms = jnp.concatenate([one, two, three], axis=1)
        for way, mask in ((0, low), (1, high)):
            sums = mm(jnp.where(mask, 1.0, 0.0).astype(BF16), terms)
            run = sums[:, 0:keyw] + sums[:, keyw : 2 * keyw] + sums[:, 2 * keyw :]
            mid_row = BLOCK // 2 - 1 if way == 0 else BLOCK // 2
            end_row = BLOCK - 1 if way == 0 else 0
            middle = run[mid_row : mid_row + 1, :]
            closing = run[end_row : end_row + 1, :]
            decs[way, 0, span, :] = jnp.exp(run)
            decs[way, 1, span, :] = jnp.exp(run - middle)
            decs[way, 2, span, :] = jnp.exp(middle - run)
            decs[way, 3, span, :] = jnp.exp(closing - run)
            ends[way, b] = jnp.broadcast_to(jnp.exp(closing), (8, keyw))

    pump()
    arrived([0])

    glide(min(blocks, n // 2 - 1), lambda tick: prepare(tick - 1))
    for b in range(min(blocks, n // 2 - 1), blocks):
        prepare(b)
    place_rows = iota(place.shape, 0)
    place_cols = iota(place.shape, 1)
    padded = g_dn.shape[2]
    place[...] = jnp.where(
        (place_rows // dn_rows == place_cols // padded)
        & (place_rows % dn_rows == place_cols % padded),
        1.0,
        0.0,
    ).astype(BF16)
    glide(starts[QKV] + final[QKV] + 1 - clock[0], lambda tick: None)
    y_arrived(QKV)

    def project(lo, hi):
        return mm(normed[...], g_qkv[:, :, lo:hi].reshape(n * depth, hi - lo)).astype(BF16)

    both = project(0, 2 * keyw)
    qs[...] = both[:, 0:keyw]
    ks[...] = both[:, keyw:]
    pump(PUMP[0])
    vs[...] = project(2 * keyw, 2 * keyw + valw)

    for b in range(blocks):
        span = slice(b * BLOCK, (b + 1) * BLOCK)
        q, k, v = qs[span, :].astype(F32), ks[span, :].astype(F32), vs[span, :]
        scores = 0.0
        for way, mask in ((0, low), (1, high)):
            pair = mm_nt(
                (q * decs[way, 1, span, :]).astype(BF16), (k * decs[way, 2, span, :]).astype(BF16)
            )
            scores = scores + jnp.where(mask, pair, 0.0)
            (ups_f, ups_b)[way][b] = mm_tn(v, (k * decs[way, 3, span, :]).astype(BF16))
        inside[span, :] = mm(scores.astype(BF16), v)
        if b % 4 == 3:
            pump(PUMP[1])
    for way, ups, blocks_in_turn in ((0, ups_f, range(blocks)), (1, ups_b, range(blocks - 1, -1, -1))):
        state = jnp.zeros((valw, keyw), F32)
        for b in blocks_in_turn:
            car[b, :, way * keyw : (way + 1) * keyw] = state.astype(BF16)
            state = state * ends[way, b, 0:1, :] + ups[b]
    complete(OUT)
    y_arrived(OUT)
    wout[...] = g_out[...].astype(F32).reshape(wout.shape).astype(BF16)
    for b in range(blocks):
        span = slice(b * BLOCK, (b + 1) * BLOCK)
        q = qs[span, :].astype(F32)
        reach = jnp.concatenate(
            [(q * decs[0, 0, span, :]).astype(BF16), (q * decs[1, 0, span, :]).astype(BF16)], axis=1
        )
        mixed = inside[span, :] + mm_nt(reach, car[b])
        headed[b] = scaled_rows(mixed, hgain_ref[...]).astype(BF16)
    pump(PUMP[2])

    low_rows, high_rows = slice(0, share // 2), slice(share // 2, share)

    def chip_rows(ref, which):
        return jnp.concatenate([ref[2 * i + which] for i in range(chips)], axis=0)

    ahead, behind = lax.rem(chip + 1, chips), lax.rem(chip + chips - 1, chips)
    across = lax.rem(chip + far, chips)

    class Sums:
        def __init__(self, bufs):
            self.bufs = bufs
            self.own, self.sent, self.got, self.tx, self.rx = bufs[:5]

        def copy(self, src, dst, sent, got, to):
            return pltpu.make_async_remote_copy(
                src_ref=src, dst_ref=dst, send_sem=sent, recv_sem=got,
                device_id={"tp": to}, device_id_type=MESH,
            )

        def ring(self, q, k):
            return self.copy(
                self.tx.at[q, k], self.rx.at[q, k], self.bufs[5].at[q, 1],
                self.bufs[6].at[q, {0: 1, 3: 2}.get(k, 3)], right if k < 3 else left,
            )

        def rings(self, q, count):
            some = pl.ds(0, count)
            return self.copy(
                self.tx.at[q, some], self.rx.at[q, some], self.bufs[5].at[q, 1],
                self.bufs[6].at[q, 3], right,
            )

        def pair(self, q):
            return self.copy(
                self.sent.at[q], self.got.at[q], self.bufs[5].at[q, 0], self.bufs[6].at[q, 0], mate
            )

        def multiply(self, q, source, weight):
            other = mm(chip_rows(source, 1 - core), weight)
            self.sent[q] = other.astype(BF16).reshape(self.sent.shape[1:])
            self.pair(q).start()
            self.own[q] = mm(chip_rows(source, core), weight).reshape(self.own.shape[1:])

        def of(self, q, which, span):
            return self.own[q, which, span, :] + self.got[q, which, span, :].astype(F32)

        def send_off(self, q):
            self.pair(q).wait_recv()
            self.tx[q, 0] = self.of(q, across, low_rows).astype(BF16)
            self.tx[q, 3] = self.of(q, across, high_rows).astype(BF16)
            self.ring(q, 0).start()
            self.ring(q, 3).start()
            self.tx[q, 1] = self.of(q, ahead, high_rows).astype(BF16)
            self.tx[q, 4] = self.of(q, behind, low_rows).astype(BF16)
            self.ring(q, 1).start()
            self.ring(q, 4).start()

        def relay(self, q):
            self.ring(q, 0).wait_recv()
            self.tx[q, 2] = (self.of(q, ahead, low_rows) + self.rx[q, 0].astype(F32)).astype(BF16)
            self.ring(q, 2).start()
            self.ring(q, 3).wait_recv()
            self.tx[q, 5] = (self.of(q, behind, high_rows) + self.rx[q, 3].astype(F32)).astype(BF16)
            self.ring(q, 5).start()

        def finish(self, q):
            self.rings(q, 4).wait_recv()
            top = self.of(q, chip, low_rows) + self.rx[q, 2].astype(F32) + self.rx[q, 4].astype(F32)
            end = self.of(q, chip, high_rows) + self.rx[q, 1].astype(F32) + self.rx[q, 5].astype(F32)
            return jnp.concatenate([top, end], axis=0)

        def drain(self, q):
            self.pair(q).wait_send()
            self.rings(q, 6).wait_send()

    mix, ff = Sums(mix_bufs), Sums(ff_bufs)

    def ag_copy(a, k, buf):
        opposite = lax.rem(t + 2 * far, tp)
        slot, span, to = [
            (t, None, mate),
            (t, None, right),
            (t, None, left),
            (left, low_rows, right),
            (right, high_rows, left),
            (left, None, mate),
            (right, None, mate),
            (opposite, low_rows, mate),
            (opposite, high_rows, mate),
        ][k]
        view = buf(slot, slice(None) if span is None else span)
        return ag_any(a, view, {1: 0, 2: 1, 3: 2, 4: 3}.get(k, 4), to)

    def ag_any(a, view, got, to):
        return pltpu.make_async_remote_copy(
            src_ref=view, dst_ref=view, send_sem=ag_send.at[a], recv_sem=ag_recv.at[a, got],
            device_id={"tp": to}, device_id_type=MESH,
        )

    def ag_drain(a, buf):
        ag_any(a, buf(pl.ds(0, tp - 1), slice(None)), 0, mate).wait_send()

    def ag_start(a, buf):
        for k in (1, 2, 0):
            ag_copy(a, k, buf).start()

    def ag_relay(a, buf):
        ag_copy(a, 1, buf).wait_recv()
        ag_copy(a, 3, buf).start()
        ag_copy(a, 5, buf).start()
        ag_copy(a, 2, buf).wait_recv()
        ag_copy(a, 4, buf).start()
        ag_copy(a, 6, buf).start()

    def ag_finish(a, buf):
        ag_copy(a, 3, buf).wait_recv()
        ag_copy(a, 7, buf).start()
        ag_copy(a, 4, buf).wait_recv()
        ag_copy(a, 8, buf).start()
        ag_any(a, buf(pl.ds(0, tp // 2), slice(None)), 4, mate).wait_recv()

    def mid_rows(slots, span):
        return full2.at[slots, span, :]

    def last_rows(c):
        return lambda slots, span: full3.at[slots, span, c * cols : (c + 1) * cols]

    for c in range(MIX_CHUNKS):
        mix.multiply(c, headed, wout[:, c * mix_cols : (c + 1) * mix_cols])
    pump(PUMP[3])
    for c in range(MIX_CHUNKS):
        mix.send_off(c)
    pump(PUMP[4])
    mix.relay(0)
    pump(PUMP[5])
    mix.relay(1)
    pump(PUMP[6])
    own_rows = pl.ds(pl.multiple_of(t * share, share), share)
    for c in range(MIX_CHUNKS):
        span = slice(c * mix_cols, (c + 1) * mix_cols)
        own_res[:, span] = (x_ref[own_rows, span].astype(F32) + mix.finish(c)).astype(BF16)
    full2[t] = scaled_rows(own_res[...].astype(F32), gain2_ref[...]).astype(BF16)
    ag_start(0, mid_rows)
    pump(PUMP[7])
    ag_relay(0, mid_rows)
    pump(PUMP[8])
    ag_finish(0, mid_rows)
    for p in GU:
        complete(p)
    for p in GU:
        y_arrived(p)

    normed2 = full2[...].reshape(rows, wide)
    for lo in range(0, 2 * ffw, 2 * LANES):
        hi = min(lo + 2 * LANES, 2 * ffw)
        wide_gu[:, lo:hi] = mm(normed2, g_gu[:, :, lo:hi].reshape(n * depth, hi - lo))
    for i in range(tp):
        span = slice(i * share, (i + 1) * share)
        tail = wide_gu[span, 2 * whole :]
        gate = jnp.concatenate([wide_gu[span, 0:whole], tail[:, 0:rest]], axis=1)
        up = jnp.concatenate([wide_gu[span, whole : 2 * whole], tail[:, rest:]], axis=1)
        hidden = (gate / (1.0 + jnp.exp(-gate)) * up).astype(BF16)
        hid[i] = mm(hidden, place[...]).astype(BF16)
    pump()

    def multiply(c):
        complete(DN[c])
        weight = g_dn[c].astype(F32).reshape(n * padded, cols).astype(BF16)
        ff.multiply(c, hid, weight)

    def finish(c):
        done = own_res[:, c * cols : (c + 1) * cols].astype(F32) + ff.finish(c)
        full3[t, :, c * cols : (c + 1) * cols] = done.astype(BF16)
        ag_start(1 + c, last_rows(c))

    def put(c):
        span = slice(c * cols, (c + 1) * cols)
        return pltpu.make_async_copy(full3.at[:, :, span], out_ref.at[:, :, span], out_sem.at[c])

    def end(c):
        ag_finish(1 + c, last_rows(c))
        put(c).start()

    stages = (multiply, ff.send_off, ff.relay, finish, lambda c: ag_relay(1 + c, last_rows(c)), end)
    idle = [functools.partial(drain, p) for p in order] + [
        functools.partial(mix.drain, c) for c in range(MIX_CHUNKS)
    ] + [functools.partial(ag_drain, 0, mid_rows)]
    for beat in range(FF_CHUNKS + len(stages) - 1):
        for k in reversed(range(len(stages))):
            if 0 <= beat - k < FF_CHUNKS:
                stages[k](beat - k)
        if beat >= FF_CHUNKS:
            for _ in range(3):
                if idle:
                    idle.pop(0)()
    for job in idle:
        job()

    for c in range(FF_CHUNKS):
        ff.drain(c)
        ag_drain(1 + c, last_rows(c))
    for c in range(FF_CHUNKS):
        put(c).wait()


def fetching(size, paired, *refs):
    count = 15
    theirs, out_ref, mine, sem = refs[:count], refs[count], refs[count + 1 : 2 * count + 1], refs[-1]

    def fetch(i):
        return pltpu.make_async_copy(theirs[i], mine[i], sem.at[i])

    for i in [*range(1, count), 0]:
        fetch(i).start()

    def arrived(some):
        for i in some:
            fetch(i).wait()

    kernel(size, paired, arrived, *mine, out_ref, *refs[2 * count + 1 : -1])


def sum_buffers(count, chips, share, cols):
    return (
        pltpu.VMEM((count, chips, share, cols), F32),
        pltpu.VMEM((count, chips, share, cols), BF16),
        pltpu.VMEM((count, chips, share, cols), BF16),
        pltpu.VMEM((count, 6, share // 2, cols), BF16),
        pltpu.VMEM((count, 6, share // 2, cols), BF16),
        pltpu.SemaphoreType.DMA((count, 2)),
        pltpu.SemaphoreType.DMA((count, 4)),
    )


def shards(size, *args):
    (x, gain1, wq, wk, wv, first, second, bias, extra, hgain, wo, gain2, wg, wu, wd) = args
    n, tp = size["fs"], size["tp"]
    paired = size["grp"] % 2 == 0
    rows, wide = x.shape
    depth, keyw = wq.shape
    valw, ffw = wv.shape[1], wg.shape[1]
    share, chips, blocks = rows // tp, tp // 2, rows // BLOCK
    cols = wide // FF_CHUNKS
    padded = -(-wd.shape[0] // 8) * 8
    sems = pltpu.SemaphoreType.DMA
    vmem = pltpu.VMEM
    steps = n // 2
    given = (
        x, gain1.reshape(1, -1), wq, wk, wv, first.T, second, bias.reshape(1, -1), extra.T,
        hgain.reshape(1, -1), wo, gain2.reshape(1, -1), wg, wu, wd,
    )
    out = pl.pallas_call(
        functools.partial(fetching, size, paired),
        out_shape=jax.ShapeDtypeStruct((tp, share, wide), BF16),
        in_specs=[pl.BlockSpec(memory_space=pltpu.HBM)] * len(given),
        out_specs=pl.BlockSpec(memory_space=pltpu.HBM),
        scratch_shapes=[vmem(a.shape, a.dtype) for a in given] + [
            vmem((n, depth, 2 * keyw + valw), BF16),
            vmem((n, wo.shape[0], wide), BF16),
            vmem((n, depth, 2 * ffw), BF16),
            vmem((FF_CHUNKS, n, padded, cols), BF16),
            vmem((rows, wide), BF16),
            vmem((rows, 1), F32),
            vmem((2, 4, rows, keyw), F32),
            vmem((2, blocks, 8, keyw), F32),
            vmem((rows, keyw), BF16),
            vmem((rows, keyw), BF16),
            vmem((rows, valw), BF16),
            vmem((rows, valw), F32),
            vmem((blocks, valw, keyw), F32),
            vmem((blocks, valw, keyw), F32),
            vmem((blocks, valw, 2 * keyw), BF16),
            vmem((blocks, BLOCK, valw), BF16),
            vmem((n * wo.shape[0], wide), BF16),
            vmem((ffw, n * padded), BF16),
            vmem((tp, share, n * padded), BF16),
            vmem((rows, 2 * ffw), F32),
            sum_buffers(MIX_CHUNKS, chips, share, wide // MIX_CHUNKS),
            sum_buffers(FF_CHUNKS, chips, share, cols),
            vmem((share, wide), BF16),
            vmem((tp, share, wide), BF16),
            vmem((tp, share, wide), BF16),
            sems((2 + len(GU_ROWS) + len(DN_SPLIT), 2)),
            sems((2 + len(GU_ROWS) + len(DN_SPLIT), 2, steps)),
            sems((2 + len(GU_ROWS),)),
            sems((2 + len(GU_ROWS),)),
            sems((1 + FF_CHUNKS,)),
            sems((1 + FF_CHUNKS, 5)),
            sems((FF_CHUNKS,)),
            sems((len(given),)),
        ],
        compiler_params=pltpu.CompilerParams(
            collective_id=0, has_side_effects=True, vmem_limit_bytes=VMEM_MIB * 1024 * 1024
        ),
        name="layer",
    )(*given)
    return out.reshape(rows, wide)


def solution(mesh):
    placed = (
        P(("grp", "fs"), None),
        P(),
        P("fs", "tp"),
        P("fs", "tp"),
        P("fs", "tp"),
        P(),
        P(None, "tp"),
        P("tp"),
        P(("grp", "fs"), "tp"),
        P(),
        P(("tp", "fs"), None),
        P(),
        P("fs", "tp"),
        P("fs", "tp"),
        P(("tp", "fs"), None),
    )
    return jax.shard_map(
        functools.partial(shards, dict(mesh.shape)),
        mesh=mesh, in_specs=placed, out_specs=P(("grp", "fs"), None), check_vma=False,
    )
```

profile of v0, /device:TPU:33, one launch (start us, length us, event | category | flops | bytes accessed | tf_op | source)
XLA Modules:
  0.0 196.7 jit_solution(13732968319638011076)
XLA Ops:
  0.0 193.6 %layer.1 = bf16[8,64,2048]{2,1,0:T(8,128)(2,1)} custom-call(bf16[512,2048]{1,0:T(8,128)(2,1)} %refs_0_.1, f32[1,2048]{1,0:T(1,128)} %bitcast.9, bf16[64,128]{1,0:T(8,128)(2,1)} %refs_2_.1, bf16[64,128]{1,0:T(8,128)(2,1)} %refs_3_.1, bf16[64,256]{1,0:T(8,128)(2,1)} %refs_4_.1, bf16[16,2048]{1,0:T(8,128)(2,1)} %bitcast.8, bf16[16,128]{1,0:T(8,128)(2,1)} %refs_6_.1, ...), custom_call_target="tpu_custom_call" | custom-call | tf_op jit(solution)/shard_map/layer/pallas_call | solution.py:592
  193.6 3.2 %copy.17 = bf16[512,2048]{1,0:T(8,128)(2,1)} copy(bf16[512,2048]{1,0:T(8,128)(2,1)} %bitcast.7) | data formatting | bytes 4194304
where the time goes:
time: 197 us
  Pallas kernels  194 us (98%)
  local copies, waits for them, and re-layouts  3.16 us (2%)
    pallas_call x1, Pallas kernels, shards(): pl.pallas_call(functools.partial(fetching, size, paired), out_shape=jax.S...  194 us

commit v1 on v0

--- a/solution.py
+++ b/solution.py
@@ -283,9 +283,6 @@
     pump()
     arrived([0])
 
-    glide(min(blocks, n // 2 - 1), lambda tick: prepare(tick - 1))
-    for b in range(min(blocks, n // 2 - 1), blocks):
-        prepare(b)
     place_rows = iota(place.shape, 0)
     place_cols = iota(place.shape, 1)
     padded = g_dn.shape[2]
@@ -297,6 +294,13 @@
     ).astype(BF16)
     glide(starts[QKV] + final[QKV] + 1 - clock[0], lambda tick: None)
     y_arrived(QKV)
+    for lo in range(0, blocks, blocks // 2):
+
+        @pl.loop(lo, lo + blocks // 2)
+        def _(b):
+            prepare(b)
+
+        pump()
 
     def project(lo, hi):
         return mm(normed[...], g_qkv[:, :, lo:hi].reshape(n * depth, hi - lo)).astype(BF16)

time: 197 us -> 198 us (level)
  no operation moved by 1% of the time
where the time goes in v1:
time: 198 us
  Pallas kernels  194 us (98%)
  local copies, waits for them, and re-layouts  3.16 us (2%)
    pallas_call x1, Pallas kernels, shards(): pl.pallas_call(functools.partial(fetching, size, paired), out_shape=jax.S...  194 us

profile of v1, /device:TPU:33, one launch (start us, length us, event | category | flops | bytes accessed | tf_op | source)
XLA Modules:
  0.0 197.6 jit_solution(9380509759618203233)
XLA Ops:
  0.0 194.4 %layer.1 = bf16[8,64,2048]{2,1,0:T(8,128)(2,1)} custom-call(bf16[512,2048]{1,0:T(8,128)(2,1)} %refs_0_.1, f32[1,2048]{1,0:T(1,128)} %bitcast.9, bf16[64,128]{1,0:T(8,128)(2,1)} %refs_2_.1, bf16[64,128]{1,0:T(8,128)(2,1)} %refs_3_.1, bf16[64,256]{1,0:T(8,128)(2,1)} %refs_4_.1, bf16[16,2048]{1,0:T(8,128)(2,1)} %bitcast.8, bf16[16,128]{1,0:T(8,128)(2,1)} %refs_6_.1, ...), custom_call_target="tpu_custom_call" | custom-call | tf_op jit(solution)/shard_map/layer/pallas_call | solution.py:596
  194.4 3.2 %copy.17 = bf16[512,2048]{1,0:T(8,128)(2,1)} copy(bf16[512,2048]{1,0:T(8,128)(2,1)} %bitcast.7) | data formatting | bytes 4194304
